TPU v7x, 32 devices: a whole 2x2x4 slice. The times are simulated.
32 devices in a mesh: ep: 8 (over z, y), tp: 4 (over x, core).
Axes of the slice: x: 2, y: 2, z: 4, core: 2. Of those that a mesh axis runs over, the one named last changes fastest.
Arguments:
- tokens: bfloat16 [2048, 2048], P('ep', 'tp'), may hold values from -72 to 72
- norm_gain: bfloat16 [2048], P('tp'), may hold values from 0.099609375 to 1.8984375
- expert_ids: int32 [2048, 2], P('ep'), may hold values from 0 to 7, all different within a row; in each aligned block of 256 rows (0 to 255, 256 to 511, ...) at most 128 rows name the same one
- gate_share: float32 [2048, 2], P('ep'), may hold values from 0.1 to 1
- gate_weight: bfloat16 [8, 2048, 4096], P('ep', None, 'tp'), may hold values from -0.125 to 0.125
- up_weight: bfloat16 [8, 2048, 4096], P('ep', None, 'tp'), may hold values from -0.125 to 0.125
- down_weight: bfloat16 [8, 4096, 2048], P('ep', 'tp'), may hold values from -0.09375 to 0.09375
Outputs:
- mixed: bfloat16 [2048, 2048], P('ep', 'tp')
Inputs may be any that keep to these rules, and one draw needn't show every extreme that they name: `expert_ids`: each token names two different experts; among the 256 tokens of one index of ep no expert is named more than 128 times, a bound that some block reaches.
All inputs are finite; a program needn't handle non-finite values.
Results may differ from a plain program's by a relative error of at most 0.019.
Values may be sent and summed in bfloat16 or wider, within the bound.
No kernel may reach another device: no remote copies, remote signals or barrier semaphores. Data moves between devices by JAX's collectives and lax.ppermute only.
A program may use at most 64 MiB of HBM per device.

v0:
```python
import functools

import jax
import jax.numpy as jnp
from jax import lax
from jax.experimental import pallas as pl
from jax.experimental.pallas import tpu as pltpu
from jax.sharding import PartitionSpec as P

EPS = 1e-06
MIB = 1024 * 1024
VMEM = pl.BlockSpec(memory_space=pltpu.VMEM)
SMEM = pl.BlockSpec(memory_space=pltpu.SMEM)
HBM = pl.BlockSpec(memory_space=pltpu.HBM)


def swap(value, axis, bits):
    n = lax.axis_size(axis)
    return lax.ppermute(value, axis, [(i, i ^ bits) for i in range(n)])


def dispatch_kernel(me_ref, ids_ref, tokens_ref, *outs):
    rows = tokens_ref.shape[0]
    cap = outs[0].shape[0]
    expert = lax.broadcasted_iota(jnp.int32, (len(outs), rows), 0) ^ me_ref[0]
    named = (ids_ref[0:1, :] == expert) | (ids_ref[1:2, :] == expert)
    earlier = lax.broadcasted_iota(jnp.int32, (rows, rows), 0) < lax.broadcasted_iota(jnp.int32, (rows, rows), 1)
    slots = jnp.dot(
        named.astype(jnp.bfloat16), earlier.astype(jnp.bfloat16), preferred_element_type=jnp.float32
    ).astype(jnp.int32)
    slots = jnp.where(named, slots, -1)
    place = lax.broadcasted_iota(jnp.int32, (cap, rows), 0)
    tokens = tokens_ref[...]
    for k, out in enumerate(outs):
        pick = (place == slots[k : k + 1, :]).astype(jnp.float32).astype(jnp.bfloat16)
        out[...] = jnp.dot(pick, tokens, preferred_element_type=jnp.float32).astype(jnp.bfloat16)


def dispatch(me, ids, tokens, n_out, cap):
    return pl.pallas_call(
        dispatch_kernel,
        out_shape=[jax.ShapeDtypeStruct((cap, tokens.shape[1]), jnp.bfloat16)] * n_out,
        in_specs=[SMEM, VMEM, VMEM],
        out_specs=[VMEM] * n_out,
        compiler_params=pltpu.CompilerParams(vmem_limit_bytes=8 * MIB),
        name="dispatch",
    )(me, ids, tokens)


def join_kernel(*refs):
    out, at = refs[-1], 0
    for ref in refs[:-1]:
        out[at : at + ref.shape[0], :] = ref[...]
        at += ref.shape[0]


def join(arrays):
    shape = (sum(a.shape[0] for a in arrays), arrays[0].shape[1])
    return pl.pallas_call(
        join_kernel,
        out_shape=jax.ShapeDtypeStruct(shape, arrays[0].dtype),
        in_specs=[VMEM] * len(arrays),
        out_specs=VMEM,
        compiler_params=pltpu.CompilerParams(vmem_limit_bytes=4 * MIB),
        name="join",
    )(*arrays)


def sum_kernel(*refs, n_in, size, blocks):
    outs = refs[n_in:]
    step = size // len(outs)
    for i, out in enumerate(outs):
        total = 0.0
        for ref, block in zip(refs, blocks):
            total = total + ref[block * size + i * step : block * size + (i + 1) * step, :].astype(jnp.float32)
        out[...] = total.astype(jnp.bfloat16)


def add_up(addends, size, n_out):
    width = addends[0][0].shape[1]
    return pl.pallas_call(
        functools.partial(sum_kernel, n_in=len(addends), size=size, blocks=[b for _, b in addends]),
        out_shape=[jax.ShapeDtypeStruct((size // n_out, width), jnp.bfloat16)] * n_out,
        in_specs=[VMEM] * len(addends),
        out_specs=[VMEM] * n_out,
        compiler_params=pltpu.CompilerParams(vmem_limit_bytes=4 * MIB),
        name="sum",
    )(*[a for a, _ in addends])


def place_kernel(me_ref, ids_ref, share_ref, target_out, share_out, *, experts, cap):
    rows = ids_ref.shape[1]
    expert = lax.broadcasted_iota(jnp.int32, (experts, rows), 0)
    chosen = [ids_ref[j : j + 1, :] == expert ^ me_ref[0] for j in range(2)]
    earlier = lax.broadcasted_iota(jnp.int32, (rows, rows), 0) < lax.broadcasted_iota(jnp.int32, (rows, rows), 1)
    named = chosen[0] | chosen[1]
    slots = jnp.dot(named.astype(jnp.bfloat16), earlier.astype(jnp.bfloat16), preferred_element_type=jnp.float32)
    target = slots + (cap * expert).astype(jnp.float32)
    lines = [jnp.sum(jnp.where(c, target, 0.0), axis=0, keepdims=True) for c in chosen]
    lines = lines + [share_ref[0:1, :], share_ref[1:2, :], jnp.zeros((4, rows), jnp.float32)]
    columns = jnp.transpose(jnp.concatenate(lines, axis=0))
    target_out[...] = columns[:, 0:2].astype(jnp.int32)
    share_out[...] = columns[:, 2:4]


def combine_kernel(target_ref, share_ref, *refs):
    blocks, out, table = refs[:-2], refs[-2], refs[-1]
    cap = blocks[0].shape[0]
    for k, block in enumerate(blocks):
        table[k * cap : (k + 1) * cap, :] = block[...]
    rows = out.shape[0]
    total = jnp.zeros(out.shape, jnp.float32)
    slot = lax.broadcasted_iota(jnp.int32, (rows, table.shape[0]), 1)
    for j in range(2):
        pick = (slot == target_ref[:, j : j + 1]).astype(jnp.float32).astype(jnp.bfloat16)
        found = jnp.dot(pick, table[...], preferred_element_type=jnp.float32)
        total = total + found * share_ref[:, j : j + 1]
    out[...] = total.astype(jnp.bfloat16)


def hold_kernel(*refs):
    copies = [pltpu.make_async_copy(refs[i], refs[3 + i], refs[-1].at[i]) for i in range(3)]
    for copy in copies:
        copy.start()
    for copy in copies:
        copy.wait()


def hold(weights):
    return pl.pallas_call(
        hold_kernel,
        out_shape=[jax.ShapeDtypeStruct(w.shape, w.dtype) for w in weights],
        in_specs=[HBM] * 3,
        out_specs=[VMEM] * 3,
        scratch_shapes=[pltpu.SemaphoreType.DMA((3,))],
        compiler_params=pltpu.CompilerParams(vmem_limit_bytes=38 * MIB),
        name="hold",
    )(*weights)


def ffn_kernel(me_ref, *refs, n_tp, rows, block):
    pieces, heads = refs[:n_tp], refs[n_tp : 2 * n_tp]
    gate_ref, up_ref, down_ref, keep_ref, give_ref, normed_ref, hidden_ref = refs[2 * n_tp :]
    me = me_ref[0]
    width = pieces[0].shape[1]
    squares = jnp.zeros((rows, 1), jnp.float32)
    for piece in pieces:
        values = piece[:rows, :].astype(jnp.float32)
        squares = squares + jnp.sum(values * values, axis=1, keepdims=True)
    factor = lax.rsqrt(squares / gate_ref.shape[0] + EPS)
    for j, (piece, head) in enumerate(zip(pieces, heads)):
        at = pl.ds(pl.multiple_of((me ^ j) * width, width), width)
        gain = head[rows : rows + 16, :].astype(jnp.float32)[0:1, :]
        normed_ref[:, at] = (piece[:rows, :].astype(jnp.float32) * factor * gain).astype(jnp.bfloat16)
    normed = normed_ref[...]
    for o in range(0, gate_ref.shape[1], block):
        gate = jnp.dot(normed, gate_ref[:, o : o + block], preferred_element_type=jnp.float32)
        upper = jnp.dot(normed, up_ref[:, o : o + block], preferred_element_type=jnp.float32)
        hidden_ref[:, o : o + block] = (gate / (1.0 + jnp.exp(-gate)) * upper).astype(jnp.bfloat16)
    hidden = hidden_ref[...]
    for j in range(n_tp):
        at = pl.ds(pl.multiple_of((me ^ j) * width, width), width)
        term = jnp.dot(hidden, down_ref[:, at], preferred_element_type=jnp.float32).astype(jnp.bfloat16)
        ref = (keep_ref, give_ref)[j & 1]
        ref[(j >> 1) * rows : ((j >> 1) + 1) * rows, :] = term


def ffn(me, rows, pieces, heads, weights):
    n_tp, width = len(pieces), pieces[0].shape[1]
    d, f = weights[0].shape
    half = jax.ShapeDtypeStruct((n_tp // 2 * rows, width), jnp.bfloat16)
    return pl.pallas_call(
        functools.partial(ffn_kernel, n_tp=n_tp, rows=rows, block=min(f, 512)),
        out_shape=[half, half],
        in_specs=[SMEM] + [VMEM] * (2 * n_tp + 3),
        out_specs=[VMEM] * 2,
        scratch_shapes=[pltpu.VMEM((rows, d), jnp.bfloat16), pltpu.VMEM((rows, f), jnp.bfloat16)],
        compiler_params=pltpu.CompilerParams(vmem_limit_bytes=10 * MIB),
        cost_estimate=pl.CostEstimate(flops=6 * rows * d * f, transcendentals=rows * f, bytes_accessed=6 * d * f),
        name="ffn",
    )(me, *pieces, *heads, *weights)


def shards(tokens, norm_gain, expert_ids, gate_share, gate_weight, up_weight, down_weight):
    n_ep, n_tp = lax.axis_size("ep"), lax.axis_size("tp")
    rows, width = tokens.shape
    experts = n_ep
    cap = 4 * rows // experts
    ep = lax.axis_index("ep").reshape(1).astype(jnp.int32)
    tp = lax.axis_index("tp").reshape(1).astype(jnp.int32)
    ep, tp = lax.optimization_barrier((ep, tp))
    bits = [1 << b for b in range(n_tp.bit_length() - 1)]
    bits.reverse()

    ids = expert_ids.T
    near = dispatch(ep, ids, tokens, n_ep, cap)
    arrived = [near[0]] + [swap(near[k], "ep", k) for k in range(1, n_ep)]

    weights = hold([gate_weight[0], up_weight[0], down_weight[0]])
    gain = jnp.broadcast_to(norm_gain.reshape(1, width), (16, width))

    place = pl.pallas_call(
        functools.partial(place_kernel, experts=experts, cap=cap),
        out_shape=(jax.ShapeDtypeStruct((rows, 2), jnp.int32), jax.ShapeDtypeStruct((rows, 2), jnp.float32)),
        in_specs=[SMEM, VMEM, VMEM],
        out_specs=(VMEM, VMEM),
        compiler_params=pltpu.CompilerParams(vmem_limit_bytes=8 * MIB),
        name="place",
    )
    target, share = place(ep, ids, gate_share.T)

    group = n_ep // 4
    back = [None] * n_ep
    for c in range(4):
        names = list(range(c * group, (c + 1) * group))
        pieces = {0: join([arrived[k] for k in names] + [gain] * (c == 0))}
        for bit in bits:
            pieces.update({o ^ bit: swap(p, "tp", bit) for o, p in pieces.items()})
        pieces = [pieces[o] for o in range(n_tp)]
        heads = heads if c else pieces
        keep, give = ffn(tp, group * cap, pieces, heads, weights)
        got = swap(give, "tp", 1)
        size = group * cap
        parts = [[(keep, i), (got, i)] for i in range(n_tp // 2)]
        while len(parts) > 1:
            bit = n_tp // len(parts)
            sent = [swap(add_up(p, size, 1)[0], "tp", bit) for p in parts[1::2]]
            parts = [p + [(s, 0)] for p, s in zip(parts[0::2], sent)]
        for k, piece in zip(names, add_up(parts[0], size, group)):
            back[k] = swap(piece, "ep", k) if k else piece

    return pl.pallas_call(
        combine_kernel,
        out_shape=jax.ShapeDtypeStruct((rows, width), jnp.bfloat16),
        in_specs=[VMEM] * (2 + n_ep),
        out_specs=VMEM,
        scratch_shapes=[pltpu.VMEM((experts * cap, width), jnp.bfloat16)],
        compiler_params=pltpu.CompilerParams(vmem_limit_bytes=8 * MIB),
        name="combine",
    )(target, share, *back)


def solution(mesh):
    in_specs = (
        P("ep", "tp"),
        P("tp"),
        P("ep", None),
        P("ep", None),
        P("ep", None, "tp"),
        P("ep", None, "tp"),
        P("ep", "tp", None),
    )
    out_specs = P("ep", "tp")

    return jax.shard_map(shards, mesh=mesh, in_specs=in_specs, out_specs=out_specs, check_vma=False)
```

profile of v0, /device:TPU:0, one launch (start us, length us, event | category | flops | bytes accessed | tf_op | source)
XLA Modules:
  0.0 108.1 jit_solution(8389651897916706371)
XLA Ops:
  2.2 3.1 %collective-permute-start = (bf16[128,512]{1,0:T(8,128)(2,1)S(1)}, bf16[128,512]{1,0:T(8,128)(2,1)S(1)}, u32[]{:S(2)}, u32[]{:S(2)}) collective-permute-start(bf16[128,512]{1,0:T(8,128)(2,1)S(1)} %get-tuple-element.41), channel_id=1, source_target_pairs={{0,4},{4,0},{8,12},{12,8},{16,20},{20,16},{24,28},{28,24},{1,5},{5... | collective-permute-start | bytes 393224 | tf_op jit(solution)/shard_map/ppermute | solution.py:19
  5.3 3.6 %collective-permute-start.25 = (bf16[128,512]{1,0:T(8,128)(2,1)S(1)}, bf16[128,512]{1,0:T(8,128)(2,1)S(1)}, u32[]{:S(2)}, u32[]{:S(2)}) collective-permute-start(bf16[128,512]{1,0:T(8,128)(2,1)S(1)} %get-tuple-element.61), channel_id=1, source_target_pairs={{0,24},{4,28},{8,16},{12,20},{16,8},{20,12},{24,0},{28,4},{1,25},{... | collective-permute-start | bytes 393224 | tf_op jit(solution)/shard_map/ppermute | solution.py:19
  9.6 1.7 %collective-permute-start.2 = (bf16[272,512]{1,0:T(8,128)(2,1)S(1)}, bf16[272,512]{1,0:T(8,128)(2,1)S(1)}, u32[]{:S(2)}, u32[]{:S(2)}) collective-permute-start(bf16[272,512]{1,0:T(8,128)(2,1)S(1)} %join.4.refs_0_.refs_4_), channel_id=1, source_target_pairs={{0,2},{1,3},{2,0},{3,1},{4,6},{5,7},{6,4},{7,5},{8,10},{9,11},{10,... | collective-permute-start | bytes 835592 | tf_op jit(solution)/shard_map/ppermute | solution.py:19
  11.3 2.8 %collective-permute-start.16 = (bf16[128,512]{1,0:T(8,128)(2,1)S(1)}, bf16[128,512]{1,0:T(8,128)(2,1)S(1)}, u32[]{:S(2)}, u32[]{:S(2)}) collective-permute-start(bf16[128,512]{1,0:T(8,128)(2,1)S(1)} %get-tuple-element.55), channel_id=1, source_target_pairs={{0,16},{4,20},{8,24},{12,28},{16,0},{20,4},{24,8},{28,12},{1,17},{... | collective-permute-start | bytes 393224 | tf_op jit(solution)/shard_map/ppermute | solution.py:19
  15.2 2.5 %collective-permute-done.26.refs_1_ = bf16[128,512]{1,0:T(8,128)(2,1)S(1)} collective-permute-done((bf16[128,512]{1,0:T(8,128)(2,1)S(1)}, bf16[128,512]{1,0:T(8,128)(2,1)S(1)}, u32[]{:S(2)}, u32[]{:S(2)}) %collective-permute-start.26) | collective-permute-done | bytes 131104 | tf_op jit(solution)/shard_map/ppermute | solution.py:19
  17.7 1.9 %collective-permute-start.28 = (bf16[256,512]{1,0:T(8,128)(2,1)S(1)}, bf16[256,512]{1,0:T(8,128)(2,1)S(1)}, u32[]{:S(2)}, u32[]{:S(2)}) collective-permute-start(bf16[256,512]{1,0:T(8,128)(2,1)S(1)} %join.7.refs_0_), channel_id=1, source_target_pairs={{0,2},{1,3},{2,0},{3,1},{4,6},{5,7},{6,4},{7,5},{8,10},{9,11},{10,... | collective-permute-start | bytes 786440 | tf_op jit(solution)/shard_map/ppermute | solution.py:19
  19.6 9.5 %collective-permute-done.16.refs_0_ = bf16[128,512]{1,0:T(8,128)(2,1)S(1)} collective-permute-done((bf16[128,512]{1,0:T(8,128)(2,1)S(1)}, bf16[128,512]{1,0:T(8,128)(2,1)S(1)}, u32[]{:S(2)}, u32[]{:S(2)}) %collective-permute-start.16) | collective-permute-done | bytes 131104 | tf_op jit(solution)/shard_map/ppermute | solution.py:19
  29.2 1.7 %collective-permute-done.17.refs_1_ = bf16[128,512]{1,0:T(8,128)(2,1)S(1)} collective-permute-done((bf16[128,512]{1,0:T(8,128)(2,1)S(1)}, bf16[128,512]{1,0:T(8,128)(2,1)S(1)}, u32[]{:S(2)}, u32[]{:S(2)}) %collective-permute-start.17) | collective-permute-done | bytes 131104 | tf_op jit(solution)/shard_map/ppermute | solution.py:19
  31.0 3.4 %collective-permute-done.7.refs_0_ = bf16[128,512]{1,0:T(8,128)(2,1)S(1)} collective-permute-done((bf16[128,512]{1,0:T(8,128)(2,1)S(1)}, bf16[128,512]{1,0:T(8,128)(2,1)S(1)}, u32[]{:S(2)}, u32[]{:S(2)}) %collective-permute-start.7) | collective-permute-done | bytes 131104 | tf_op jit(solution)/shard_map/ppermute | solution.py:19
  35.0 1.8 %collective-permute-done.8.refs_1_ = bf16[128,512]{1,0:T(8,128)(2,1)S(1)} collective-permute-done((bf16[128,512]{1,0:T(8,128)(2,1)S(1)}, bf16[128,512]{1,0:T(8,128)(2,1)S(1)}, u32[]{:S(2)}, u32[]{:S(2)}) %collective-permute-start.8) | collective-permute-done | bytes 131104 | tf_op jit(solution)/shard_map/ppermute | solution.py:19
  36.8 1.6 %collective-permute-start.19 = (bf16[256,512]{1,0:T(8,128)(2,1)S(1)}, bf16[256,512]{1,0:T(8,128)(2,1)S(1)}, u32[]{:S(2)}, u32[]{:S(2)}) collective-permute-start(bf16[256,512]{1,0:T(8,128)(2,1)S(1)} %join.6.refs_0_), channel_id=1, source_target_pairs={{0,2},{1,3},{2,0},{3,1},{4,6},{5,7},{6,4},{7,5},{8,10},{9,11},{10,... | collective-permute-start | bytes 786440 | tf_op jit(solution)/shard_map/ppermute | solution.py:19
  38.9 4.7 %hold.1 = (bf16[2048,1024]{1,0:T(8,128)(2,1)S(1)}, bf16[2048,1024]{1,0:T(8,128)(2,1)S(1)}, bf16[1024,2048]{1,0:T(8,128)(2,1)S(1)}) custom-call(bf16[2048,1024]{1,0:T(8,128)(2,1)} %bitcast.10, bf16[2048,1024]{1,0:T(8,128)(2,1)} %bitcast.11, bf16[1024,2048]{1,0:T(8,128)(2,1)} %bitcast.12), custom_call_target="tpu_custom_call" | custom-call | tf_op jit(solution)/shard_map/hold/pallas_call | solution.py:130
  43.6 2.4 %collective-permute-done.19.refs_2_ = bf16[256,512]{1,0:T(8,128)(2,1)S(1)} collective-permute-done((bf16[256,512]{1,0:T(8,128)(2,1)S(1)}, bf16[256,512]{1,0:T(8,128)(2,1)S(1)}, u32[]{:S(2)}, u32[]{:S(2)}) %collective-permute-start.19) | collective-permute-done | bytes 262176 | tf_op jit(solution)/shard_map/ppermute | solution.py:19
  45.9 3.4 %collective-permute-done.10.refs_2_ = bf16[256,512]{1,0:T(8,128)(2,1)S(1)} collective-permute-done((bf16[256,512]{1,0:T(8,128)(2,1)S(1)}, bf16[256,512]{1,0:T(8,128)(2,1)S(1)}, u32[]{:S(2)}, u32[]{:S(2)}) %collective-permute-start.10) | collective-permute-done | bytes 262176 | tf_op jit(solution)/shard_map/ppermute | solution.py:19
  49.9 4.0 %ffn.7 = (bf16[512,512]{1,0:T(8,128)(2,1)S(1)}, bf16[512,512]{1,0:T(8,128)(2,1)S(1)}) custom-call(s32[1]{0:T(128)} %bitcast.1.me_ref, bf16[256,512]{1,0:T(8,128)(2,1)S(1)} %join.7.refs_0_, bf16[256,512]{1,0:T(8,128)(2,1)S(1)} %collective-permute-done.27.refs_1_, bf16[256,512]{1,0:T(8,128)(2,1)S(1)} %collective-permute-done.28.refs_2_, ...), custom_call_target="tpu_custom_call" | custom-call | flops 3221225472 | bytes 12582912 | tf_op jit(solution)/shard_map/ffn/pallas_call | solution.py:172
  54.4 4.0 %ffn.6 = (bf16[512,512]{1,0:T(8,128)(2,1)S(1)}, bf16[512,512]{1,0:T(8,128)(2,1)S(1)}) custom-call(s32[1]{0:T(128)} %bitcast.1.me_ref, bf16[256,512]{1,0:T(8,128)(2,1)S(1)} %join.6.refs_0_, bf16[256,512]{1,0:T(8,128)(2,1)S(1)} %collective-permute-done.18.refs_1_, bf16[256,512]{1,0:T(8,128)(2,1)S(1)} %collective-permute-done.19.refs_2_, ...), custom_call_target="tpu_custom_call" | custom-call | flops 3221225472 | bytes 12582912 | tf_op jit(solution)/shard_map/ffn/pallas_call | solution.py:172
  58.6 4.0 %ffn.5 = (bf16[512,512]{1,0:T(8,128)(2,1)S(1)}, bf16[512,512]{1,0:T(8,128)(2,1)S(1)}) custom-call(s32[1]{0:T(128)} %bitcast.1.me_ref, bf16[256,512]{1,0:T(8,128)(2,1)S(1)} %join.5.refs_0_, bf16[256,512]{1,0:T(8,128)(2,1)S(1)} %collective-permute-done.9.refs_1_, bf16[256,512]{1,0:T(8,128)(2,1)S(1)} %collective-permute-done.10.refs_2_, ...), custom_call_target="tpu_custom_call" | custom-call | flops 3221225472 | bytes 12582912 | tf_op jit(solution)/shard_map/ffn/pallas_call | solution.py:172
  63.1 4.2 %ffn.4 = (bf16[512,512]{1,0:T(8,128)(2,1)S(1)}, bf16[512,512]{1,0:T(8,128)(2,1)S(1)}) custom-call(s32[1]{0:T(128)} %bitcast.1.me_ref, bf16[272,512]{1,0:T(8,128)(2,1)S(1)} %join.4.refs_0_.refs_4_, bf16[272,512]{1,0:T(8,128)(2,1)S(1)} %collective-permute-done.1.refs_1_.refs_5_, bf16[272,512]{1,0:T(8,128)(2,1)S(1)} %collective-permute-done.2.refs_2_.refs_6_, ...), custom_call_target="tpu_custom_call" | custom-call | flops 3221225472 | bytes 12582912 | tf_op jit(solution)/shard_map/ffn/pallas_call | solution.py:172
  69.8 1.3 %collective-permute-start.13 = (bf16[256,512]{1,0:T(8,128)(2,1)S(1)}, bf16[256,512]{1,0:T(8,128)(2,1)S(1)}, u32[]{:S(2)}, u32[]{:S(2)}) collective-permute-start(bf16[256,512]{1,0:T(8,128)(2,1)S(1)} %sum.10), channel_id=1, source_target_pairs={{0,2},{1,3},{2,0},{3,1},{4,6},{5,7},{6,4},{7,5},{8,10},{9,11},{10,... | collective-permute-start | bytes 786440 | tf_op jit(solution)/shard_map/ppermute | solution.py:19
  72.0 4.7 %collective-permute-done.31.refs_2_ = bf16[256,512]{1,0:T(8,128)(2,1)S(1)} collective-permute-done((bf16[256,512]{1,0:T(8,128)(2,1)S(1)}, bf16[256,512]{1,0:T(8,128)(2,1)S(1)}, u32[]{:S(2)}, u32[]{:S(2)}) %collective-permute-start.31) | collective-permute-done | bytes 262176 | tf_op jit(solution)/shard_map/ppermute | solution.py:19
  76.8 3.3 %collective-permute-start.32 = (bf16[128,512]{1,0:T(8,128)(2,1)S(1)}, bf16[128,512]{1,0:T(8,128)(2,1)S(1)}, u32[]{:S(2)}, u32[]{:S(2)}) collective-permute-start(bf16[128,512]{1,0:T(8,128)(2,1)S(1)} %get-tuple-element.65), channel_id=1, source_target_pairs={{0,24},{4,28},{8,16},{12,20},{16,8},{20,12},{24,0},{28,4},{1,25},{... | collective-permute-start | bytes 393224 | tf_op jit(solution)/shard_map/ppermute | solution.py:19
  80.1 1.3 %collective-permute-start.33 = (bf16[128,512]{1,0:T(8,128)(2,1)S(1)}, bf16[128,512]{1,0:T(8,128)(2,1)S(1)}, u32[]{:S(2)}, u32[]{:S(2)}) collective-permute-start(bf16[128,512]{1,0:T(8,128)(2,1)S(1)} %get-tuple-element.66), channel_id=1, source_target_pairs={{0,28},{4,24},{8,20},{12,16},{16,12},{20,8},{24,4},{28,0},{1,29},{... | collective-permute-start | bytes 393224 | tf_op jit(solution)/shard_map/ppermute | solution.py:19
  82.4 3.7 %collective-permute-start.23 = (bf16[128,512]{1,0:T(8,128)(2,1)S(1)}, bf16[128,512]{1,0:T(8,128)(2,1)S(1)}, u32[]{:S(2)}, u32[]{:S(2)}) collective-permute-start(bf16[128,512]{1,0:T(8,128)(2,1)S(1)} %get-tuple-element.59), channel_id=1, source_target_pairs={{0,16},{4,20},{8,24},{12,28},{16,0},{20,4},{24,8},{28,12},{1,17},{... | collective-permute-start | bytes 393224 | tf_op jit(solution)/shard_map/ppermute | solution.py:19
  86.1 1.8 %collective-permute-done.13.refs_2_ = bf16[256,512]{1,0:T(8,128)(2,1)S(1)} collective-permute-done((bf16[256,512]{1,0:T(8,128)(2,1)S(1)}, bf16[256,512]{1,0:T(8,128)(2,1)S(1)}, u32[]{:S(2)}, u32[]{:S(2)}) %collective-permute-start.13) | collective-permute-done | bytes 262176 | tf_op jit(solution)/shard_map/ppermute | solution.py:19
  87.9 2.9 %collective-permute-start.24 = (bf16[128,512]{1,0:T(8,128)(2,1)S(1)}, bf16[128,512]{1,0:T(8,128)(2,1)S(1)}, u32[]{:S(2)}, u32[]{:S(2)}) collective-permute-start(bf16[128,512]{1,0:T(8,128)(2,1)S(1)} %get-tuple-element.60), channel_id=1, source_target_pairs={{0,20},{4,16},{8,28},{12,24},{16,4},{20,0},{24,12},{28,8},{1,21},{... | collective-permute-start | bytes 393224 | tf_op jit(solution)/shard_map/ppermute | solution.py:19
  90.9 2.1 %collective-permute-done.5.refs_2_ = bf16[256,512]{1,0:T(8,128)(2,1)S(1)} collective-permute-done((bf16[256,512]{1,0:T(8,128)(2,1)S(1)}, bf16[256,512]{1,0:T(8,128)(2,1)S(1)}, u32[]{:S(2)}, u32[]{:S(2)}) %collective-permute-start.5) | collective-permute-done | bytes 262176 | tf_op jit(solution)/shard_map/ppermute | solution.py:19
  93.0 2.2 %collective-permute-start.14 = (bf16[128,512]{1,0:T(8,128)(2,1)S(1)}, bf16[128,512]{1,0:T(8,128)(2,1)S(1)}, u32[]{:S(2)}, u32[]{:S(2)}) collective-permute-start(bf16[128,512]{1,0:T(8,128)(2,1)S(1)} %get-tuple-element.53), channel_id=1, source_target_pairs={{0,8},{4,12},{8,0},{12,4},{16,24},{20,28},{24,16},{28,20},{1,9},{5... | collective-permute-start | bytes 393224 | tf_op jit(solution)/shard_map/ppermute | solution.py:19
  97.2 3.2 %collective-permute-done.23.refs_4_ = bf16[128,512]{1,0:T(8,128)(2,1)S(1)} collective-permute-done((bf16[128,512]{1,0:T(8,128)(2,1)S(1)}, bf16[128,512]{1,0:T(8,128)(2,1)S(1)}, u32[]{:S(2)}, u32[]{:S(2)}) %collective-permute-start.23) | collective-permute-done | bytes 131104 | tf_op jit(solution)/shard_map/ppermute | solution.py:19
  100.4 1.9 %collective-permute-done.24.refs_5_ = bf16[128,512]{1,0:T(8,128)(2,1)S(1)} collective-permute-done((bf16[128,512]{1,0:T(8,128)(2,1)S(1)}, bf16[128,512]{1,0:T(8,128)(2,1)S(1)}, u32[]{:S(2)}, u32[]{:S(2)}) %collective-permute-start.24) | collective-permute-done | bytes 131104 | tf_op jit(solution)/shard_map/ppermute | solution.py:19
  102.3 2.8 %collective-permute-done.14.refs_2_ = bf16[128,512]{1,0:T(8,128)(2,1)S(1)} collective-permute-done((bf16[128,512]{1,0:T(8,128)(2,1)S(1)}, bf16[128,512]{1,0:T(8,128)(2,1)S(1)}, u32[]{:S(2)}, u32[]{:S(2)}) %collective-permute-start.14) | collective-permute-done | bytes 131104 | tf_op jit(solution)/shard_map/ppermute | solution.py:19
  105.1 1.5 %collective-permute-done.15.refs_3_ = bf16[128,512]{1,0:T(8,128)(2,1)S(1)} collective-permute-done((bf16[128,512]{1,0:T(8,128)(2,1)S(1)}, bf16[128,512]{1,0:T(8,128)(2,1)S(1)}, u32[]{:S(2)}, u32[]{:S(2)}) %collective-permute-start.15) | collective-permute-done | bytes 131104 | tf_op jit(solution)/shard_map/ppermute | solution.py:19
  106.6 1.5 %combine.1 = bf16[256,512]{1,0:T(8,128)(2,1)} custom-call(s32[256,2]{1,0:T(8,128)S(1)} %get-tuple-element.37.target_ref, f32[256,2]{1,0:T(8,128)S(1)} %get-tuple-element.38.share_ref, bf16[128,512]{1,0:T(8,128)(2,1)S(1)} %get-tuple-element.47.refs_0_, bf16[128,512]{1,0:T(8,128)(2,1)S(1)} %collective-permute-done.6.refs_1_, ...), custom_call_target="tpu_custom_call" | custom-call | tf_op jit(solution)/shard_map/combine/pallas_call | solution.py:232
  (65 shorter events, 14.0 us)
Async XLA Ops:
  2.2 6.7 %collective-permute-start = (bf16[128,512]{1,0:T(8,128)(2,1)S(1)}, bf16[128,512]{1,0:T(8,128)(2,1)S(1)}, u32[]{:S(2)}, u32[]{:S(2)}) collective-permute-start(bf16[128,512]{1,0:T(8,128)(2,1)S(1)} %get-tuple-element.41), channel_id=1, source_target_pairs={{0,4},{4,0},{8,12},{12,8},{16,20},{20,16},{24,28},{28,24},{1,5},{5... | collective-permute-start | bytes 393224 | tf_op jit(solution)/shard_map/ppermute | solution.py:19
  5.3 9.9 %collective-permute-start.25 = (bf16[128,512]{1,0:T(8,128)(2,1)S(1)}, bf16[128,512]{1,0:T(8,128)(2,1)S(1)}, u32[]{:S(2)}, u32[]{:S(2)}) collective-permute-start(bf16[128,512]{1,0:T(8,128)(2,1)S(1)} %get-tuple-element.61), channel_id=1, source_target_pairs={{0,24},{4,28},{8,16},{12,20},{16,8},{20,12},{24,0},{28,4},{1,25},{... | collective-permute-start | bytes 393224 | tf_op jit(solution)/shard_map/ppermute | solution.py:19
  8.9 8.8 %collective-permute-start.26 = (bf16[128,512]{1,0:T(8,128)(2,1)S(1)}, bf16[128,512]{1,0:T(8,128)(2,1)S(1)}, u32[]{:S(2)}, u32[]{:S(2)}) collective-permute-start(bf16[128,512]{1,0:T(8,128)(2,1)S(1)} %get-tuple-element.62), channel_id=1, source_target_pairs={{0,28},{4,24},{8,20},{12,16},{16,12},{20,8},{24,4},{28,0},{1,29},{... | collective-permute-start | bytes 393224 | tf_op jit(solution)/shard_map/ppermute | solution.py:19
  9.6 24.9 %collective-permute-start.2 = (bf16[272,512]{1,0:T(8,128)(2,1)S(1)}, bf16[272,512]{1,0:T(8,128)(2,1)S(1)}, u32[]{:S(2)}, u32[]{:S(2)}) collective-permute-start(bf16[272,512]{1,0:T(8,128)(2,1)S(1)} %join.4.refs_0_.refs_4_), channel_id=1, source_target_pairs={{0,2},{1,3},{2,0},{3,1},{4,6},{5,7},{6,4},{7,5},{8,10},{9,11},{10,... | collective-permute-start | bytes 835592 | tf_op jit(solution)/shard_map/ppermute | solution.py:19
  11.3 17.7 %collective-permute-start.16 = (bf16[128,512]{1,0:T(8,128)(2,1)S(1)}, bf16[128,512]{1,0:T(8,128)(2,1)S(1)}, u32[]{:S(2)}, u32[]{:S(2)}) collective-permute-start(bf16[128,512]{1,0:T(8,128)(2,1)S(1)} %get-tuple-element.55), channel_id=1, source_target_pairs={{0,16},{4,20},{8,24},{12,28},{16,0},{20,4},{24,8},{28,12},{1,17},{... | collective-permute-start | bytes 393224 | tf_op jit(solution)/shard_map/ppermute | solution.py:19
  14.1 16.8 %collective-permute-start.17 = (bf16[128,512]{1,0:T(8,128)(2,1)S(1)}, bf16[128,512]{1,0:T(8,128)(2,1)S(1)}, u32[]{:S(2)}, u32[]{:S(2)}) collective-permute-start(bf16[128,512]{1,0:T(8,128)(2,1)S(1)} %get-tuple-element.56), channel_id=1, source_target_pairs={{0,20},{4,16},{8,28},{12,24},{16,4},{20,0},{24,12},{28,8},{1,21},{... | collective-permute-start | bytes 393224 | tf_op jit(solution)/shard_map/ppermute | solution.py:19
  17.7 20.7 %collective-permute-start.28 = (bf16[256,512]{1,0:T(8,128)(2,1)S(1)}, bf16[256,512]{1,0:T(8,128)(2,1)S(1)}, u32[]{:S(2)}, u32[]{:S(2)}) collective-permute-start(bf16[256,512]{1,0:T(8,128)(2,1)S(1)} %join.7.refs_0_), channel_id=1, source_target_pairs={{0,2},{1,3},{2,0},{3,1},{4,6},{5,7},{6,4},{7,5},{8,10},{9,11},{10,... | collective-permute-start | bytes 786440 | tf_op jit(solution)/shard_map/ppermute | solution.py:19
  19.6 19.3 %collective-permute-start.27 = (bf16[256,512]{1,0:T(8,128)(2,1)S(1)}, bf16[256,512]{1,0:T(8,128)(2,1)S(1)}, u32[]{:S(2)}, u32[]{:S(2)}) collective-permute-start(bf16[256,512]{1,0:T(8,128)(2,1)S(1)} %join.7.refs_0_), channel_id=1, source_target_pairs={{0,1},{1,0},{2,3},{3,2},{4,5},{5,4},{6,7},{7,6},{8,9},{9,8},{10,11... | collective-permute-start | bytes 786440 | tf_op jit(solution)/shard_map/ppermute | solution.py:19
  29.1 5.4 %collective-permute-start.7 = (bf16[128,512]{1,0:T(8,128)(2,1)S(1)}, bf16[128,512]{1,0:T(8,128)(2,1)S(1)}, u32[]{:S(2)}, u32[]{:S(2)}) collective-permute-start(bf16[128,512]{1,0:T(8,128)(2,1)S(1)} %get-tuple-element.49), channel_id=1, source_target_pairs={{0,8},{4,12},{8,0},{12,4},{16,24},{20,28},{24,16},{28,20},{1,9},{5... | collective-permute-start | bytes 393224 | tf_op jit(solution)/shard_map/ppermute | solution.py:19
  30.9 5.9 %collective-permute-start.8 = (bf16[128,512]{1,0:T(8,128)(2,1)S(1)}, bf16[128,512]{1,0:T(8,128)(2,1)S(1)}, u32[]{:S(2)}, u32[]{:S(2)}) collective-permute-start(bf16[128,512]{1,0:T(8,128)(2,1)S(1)} %get-tuple-element.50), channel_id=1, source_target_pairs={{0,12},{4,8},{8,4},{12,0},{16,28},{20,24},{24,20},{28,16},{1,13},{... | collective-permute-start | bytes 393224 | tf_op jit(solution)/shard_map/ppermute | solution.py:19
  34.5 14.9 %collective-permute-start.1 = (bf16[272,512]{1,0:T(8,128)(2,1)S(1)}, bf16[272,512]{1,0:T(8,128)(2,1)S(1)}, u32[]{:S(2)}, u32[]{:S(2)}) collective-permute-start(bf16[272,512]{1,0:T(8,128)(2,1)S(1)} %join.4.refs_0_.refs_4_), channel_id=1, source_target_pairs={{0,1},{1,0},{2,3},{3,2},{4,5},{5,4},{6,7},{7,6},{8,9},{9,8},{10,11... | collective-permute-start | bytes 835592 | tf_op jit(solution)/shard_map/ppermute | solution.py:19
  34.5 15.4 %collective-permute-start.3 = (bf16[272,512]{1,0:T(8,128)(2,1)S(1)}, bf16[272,512]{1,0:T(8,128)(2,1)S(1)}, u32[]{:S(2)}, u32[]{:S(2)}) collective-permute-start(bf16[272,512]{1,0:T(8,128)(2,1)S(1)} %collective-permute-done.2.refs_2_.refs_6_), channel_id=1, source_target_pairs={{0,1},{1,0},{2,3},{3,2},{4,5},{5,4},{6,7},{7,6},{8,9},{9,8},{10,11... | collective-permute-start | bytes 835592 | tf_op jit(solution)/shard_map/ppermute | solution.py:19
  36.8 9.2 %collective-permute-start.19 = (bf16[256,512]{1,0:T(8,128)(2,1)S(1)}, bf16[256,512]{1,0:T(8,128)(2,1)S(1)}, u32[]{:S(2)}, u32[]{:S(2)}) collective-permute-start(bf16[256,512]{1,0:T(8,128)(2,1)S(1)} %join.6.refs_0_), channel_id=1, source_target_pairs={{0,2},{1,3},{2,0},{3,1},{4,6},{5,7},{6,4},{7,5},{8,10},{9,11},{10,... | collective-permute-start | bytes 786440 | tf_op jit(solution)/shard_map/ppermute | solution.py:19
  38.3 11.0 %collective-permute-start.10 = (bf16[256,512]{1,0:T(8,128)(2,1)S(1)}, bf16[256,512]{1,0:T(8,128)(2,1)S(1)}, u32[]{:S(2)}, u32[]{:S(2)}) collective-permute-start(bf16[256,512]{1,0:T(8,128)(2,1)S(1)} %join.5.refs_0_), channel_id=1, source_target_pairs={{0,2},{1,3},{2,0},{3,1},{4,6},{5,7},{6,4},{7,5},{8,10},{9,11},{10,... | collective-permute-start | bytes 786440 | tf_op jit(solution)/shard_map/ppermute | solution.py:19
  38.9 10.9 %collective-permute-start.29 = (bf16[256,512]{1,0:T(8,128)(2,1)S(1)}, bf16[256,512]{1,0:T(8,128)(2,1)S(1)}, u32[]{:S(2)}, u32[]{:S(2)}) collective-permute-start(bf16[256,512]{1,0:T(8,128)(2,1)S(1)} %collective-permute-done.28.refs_2_), channel_id=1, source_target_pairs={{0,1},{1,0},{2,3},{3,2},{4,5},{5,4},{6,7},{7,6},{8,9},{9,8},{10,11... | collective-permute-start | bytes 786440 | tf_op jit(solution)/shard_map/ppermute | solution.py:19
  45.9 8.5 %collective-permute-start.18 = (bf16[256,512]{1,0:T(8,128)(2,1)S(1)}, bf16[256,512]{1,0:T(8,128)(2,1)S(1)}, u32[]{:S(2)}, u32[]{:S(2)}) collective-permute-start(bf16[256,512]{1,0:T(8,128)(2,1)S(1)} %join.6.refs_0_), channel_id=1, source_target_pairs={{0,1},{1,0},{2,3},{3,2},{4,5},{5,4},{6,7},{7,6},{8,9},{9,8},{10,11... | collective-permute-start | bytes 786440 | tf_op jit(solution)/shard_map/ppermute | solution.py:19
  49.3 9.2 %collective-permute-start.9 = (bf16[256,512]{1,0:T(8,128)(2,1)S(1)}, bf16[256,512]{1,0:T(8,128)(2,1)S(1)}, u32[]{:S(2)}, u32[]{:S(2)}) collective-permute-start(bf16[256,512]{1,0:T(8,128)(2,1)S(1)} %join.5.refs_0_), channel_id=1, source_target_pairs={{0,1},{1,0},{2,3},{3,2},{4,5},{5,4},{6,7},{7,6},{8,9},{9,8},{10,11... | collective-permute-start | bytes 786440 | tf_op jit(solution)/shard_map/ppermute | solution.py:19
  49.8 8.7 %collective-permute-start.11 = (bf16[256,512]{1,0:T(8,128)(2,1)S(1)}, bf16[256,512]{1,0:T(8,128)(2,1)S(1)}, u32[]{:S(2)}, u32[]{:S(2)}) collective-permute-start(bf16[256,512]{1,0:T(8,128)(2,1)S(1)} %collective-permute-done.10.refs_2_), channel_id=1, source_target_pairs={{0,1},{1,0},{2,3},{3,2},{4,5},{5,4},{6,7},{7,6},{8,9},{9,8},{10,11... | collective-permute-start | bytes 786440 | tf_op jit(solution)/shard_map/ppermute | solution.py:19
  53.9 13.5 %collective-permute-start.30 = (bf16[512,512]{1,0:T(8,128)(2,1)S(1)}, bf16[512,512]{1,0:T(8,128)(2,1)S(1)}, u32[]{:S(2)}, u32[]{:S(2)}) collective-permute-start(bf16[512,512]{1,0:T(8,128)(2,1)S(1)} %get-tuple-element.64), channel_id=1, source_target_pairs={{0,1},{1,0},{2,3},{3,2},{4,5},{5,4},{6,7},{7,6},{8,9},{9,8},{10,11... | collective-permute-start | bytes 1572872 | tf_op jit(solution)/shard_map/ppermute | solution.py:19
  58.4 10.3 %collective-permute-start.21 = (bf16[512,512]{1,0:T(8,128)(2,1)S(1)}, bf16[512,512]{1,0:T(8,128)(2,1)S(1)}, u32[]{:S(2)}, u32[]{:S(2)}) collective-permute-start(bf16[512,512]{1,0:T(8,128)(2,1)S(1)} %get-tuple-element.58), channel_id=1, source_target_pairs={{0,1},{1,0},{2,3},{3,2},{4,5},{5,4},{6,7},{7,6},{8,9},{9,8},{10,11... | collective-permute-start | bytes 1572872 | tf_op jit(solution)/shard_map/ppermute | solution.py:19
  62.6 7.1 %collective-permute-start.12 = (bf16[512,512]{1,0:T(8,128)(2,1)S(1)}, bf16[512,512]{1,0:T(8,128)(2,1)S(1)}, u32[]{:S(2)}, u32[]{:S(2)}) collective-permute-start(bf16[512,512]{1,0:T(8,128)(2,1)S(1)} %get-tuple-element.52), channel_id=1, source_target_pairs={{0,1},{1,0},{2,3},{3,2},{4,5},{5,4},{6,7},{7,6},{8,9},{9,8},{10,11... | collective-permute-start | bytes 1572872 | tf_op jit(solution)/shard_map/ppermute | solution.py:19
  67.4 9.2 %collective-permute-start.31 = (bf16[256,512]{1,0:T(8,128)(2,1)S(1)}, bf16[256,512]{1,0:T(8,128)(2,1)S(1)}, u32[]{:S(2)}, u32[]{:S(2)}) collective-permute-start(bf16[256,512]{1,0:T(8,128)(2,1)S(1)} %sum.14), channel_id=1, source_target_pairs={{0,2},{1,3},{2,0},{3,1},{4,6},{5,7},{6,4},{7,5},{8,10},{9,11},{10,... | collective-permute-start | bytes 786440 | tf_op jit(solution)/shard_map/ppermute | solution.py:19
  68.8 13.5 %collective-permute-start.22 = (bf16[256,512]{1,0:T(8,128)(2,1)S(1)}, bf16[256,512]{1,0:T(8,128)(2,1)S(1)}, u32[]{:S(2)}, u32[]{:S(2)}) collective-permute-start(bf16[256,512]{1,0:T(8,128)(2,1)S(1)} %sum.12), channel_id=1, source_target_pairs={{0,2},{1,3},{2,0},{3,1},{4,6},{5,7},{6,4},{7,5},{8,10},{9,11},{10,... | collective-permute-start | bytes 786440 | tf_op jit(solution)/shard_map/ppermute | solution.py:19
  69.8 18.2 %collective-permute-start.13 = (bf16[256,512]{1,0:T(8,128)(2,1)S(1)}, bf16[256,512]{1,0:T(8,128)(2,1)S(1)}, u32[]{:S(2)}, u32[]{:S(2)}) collective-permute-start(bf16[256,512]{1,0:T(8,128)(2,1)S(1)} %sum.10), channel_id=1, source_target_pairs={{0,2},{1,3},{2,0},{3,1},{4,6},{5,7},{6,4},{7,5},{8,10},{9,11},{10,... | collective-permute-start | bytes 786440 | tf_op jit(solution)/shard_map/ppermute | solution.py:19
  71.1 21.9 %collective-permute-start.5 = (bf16[256,512]{1,0:T(8,128)(2,1)S(1)}, bf16[256,512]{1,0:T(8,128)(2,1)S(1)}, u32[]{:S(2)}, u32[]{:S(2)}) collective-permute-start(bf16[256,512]{1,0:T(8,128)(2,1)S(1)} %sum.8), channel_id=1, source_target_pairs={{0,2},{1,3},{2,0},{3,1},{4,6},{5,7},{6,4},{7,5},{8,10},{9,11},{10,... | collective-permute-start | bytes 786440 | tf_op jit(solution)/shard_map/ppermute | solution.py:19
  76.8 18.5 %collective-permute-start.32 = (bf16[128,512]{1,0:T(8,128)(2,1)S(1)}, bf16[128,512]{1,0:T(8,128)(2,1)S(1)}, u32[]{:S(2)}, u32[]{:S(2)}) collective-permute-start(bf16[128,512]{1,0:T(8,128)(2,1)S(1)} %get-tuple-element.65), channel_id=1, source_target_pairs={{0,24},{4,28},{8,16},{12,20},{16,8},{20,12},{24,0},{28,4},{1,25},{... | collective-permute-start | bytes 393224 | tf_op jit(solution)/shard_map/ppermute | solution.py:19
  80.1 15.8 %collective-permute-start.33 = (bf16[128,512]{1,0:T(8,128)(2,1)S(1)}, bf16[128,512]{1,0:T(8,128)(2,1)S(1)}, u32[]{:S(2)}, u32[]{:S(2)}) collective-permute-start(bf16[128,512]{1,0:T(8,128)(2,1)S(1)} %get-tuple-element.66), channel_id=1, source_target_pairs={{0,28},{4,24},{8,20},{12,16},{16,12},{20,8},{24,4},{28,0},{1,29},{... | collective-permute-start | bytes 393224 | tf_op jit(solution)/shard_map/ppermute | solution.py:19
  82.4 18.0 %collective-permute-start.23 = (bf16[128,512]{1,0:T(8,128)(2,1)S(1)}, bf16[128,512]{1,0:T(8,128)(2,1)S(1)}, u32[]{:S(2)}, u32[]{:S(2)}) collective-permute-start(bf16[128,512]{1,0:T(8,128)(2,1)S(1)} %get-tuple-element.59), channel_id=1, source_target_pairs={{0,16},{4,20},{8,24},{12,28},{16,0},{20,4},{24,8},{28,12},{1,17},{... | collective-permute-start | bytes 393224 | tf_op jit(solution)/shard_map/ppermute | solution.py:19
  87.9 14.4 %collective-permute-start.24 = (bf16[128,512]{1,0:T(8,128)(2,1)S(1)}, bf16[128,512]{1,0:T(8,128)(2,1)S(1)}, u32[]{:S(2)}, u32[]{:S(2)}) collective-permute-start(bf16[128,512]{1,0:T(8,128)(2,1)S(1)} %get-tuple-element.60), channel_id=1, source_target_pairs={{0,20},{4,16},{8,28},{12,24},{16,4},{20,0},{24,12},{28,8},{1,21},{... | collective-permute-start | bytes 393224 | tf_op jit(solution)/shard_map/ppermute | solution.py:19
  93.0 12.1 %collective-permute-start.14 = (bf16[128,512]{1,0:T(8,128)(2,1)S(1)}, bf16[128,512]{1,0:T(8,128)(2,1)S(1)}, u32[]{:S(2)}, u32[]{:S(2)}) collective-permute-start(bf16[128,512]{1,0:T(8,128)(2,1)S(1)} %get-tuple-element.53), channel_id=1, source_target_pairs={{0,8},{4,12},{8,0},{12,4},{16,24},{20,28},{24,16},{28,20},{1,9},{5... | collective-permute-start | bytes 393224 | tf_op jit(solution)/shard_map/ppermute | solution.py:19
  95.3 11.3 %collective-permute-start.15 = (bf16[128,512]{1,0:T(8,128)(2,1)S(1)}, bf16[128,512]{1,0:T(8,128)(2,1)S(1)}, u32[]{:S(2)}, u32[]{:S(2)}) collective-permute-start(bf16[128,512]{1,0:T(8,128)(2,1)S(1)} %get-tuple-element.54), channel_id=1, source_target_pairs={{0,12},{4,8},{8,4},{12,0},{16,28},{20,24},{24,20},{28,16},{1,13},{... | collective-permute-start | bytes 393224 | tf_op jit(solution)/shard_map/ppermute | solution.py:19
  95.9 10.8 %collective-permute-start.6 = (bf16[128,512]{1,0:T(8,128)(2,1)S(1)}, bf16[128,512]{1,0:T(8,128)(2,1)S(1)}, u32[]{:S(2)}, u32[]{:S(2)}) collective-permute-start(bf16[128,512]{1,0:T(8,128)(2,1)S(1)} %get-tuple-element.48), channel_id=1, source_target_pairs={{0,4},{4,0},{8,12},{12,8},{16,20},{20,16},{24,28},{28,24},{1,5},{5... | collective-permute-start | bytes 393224 | tf_op jit(solution)/shard_map/ppermute | solution.py:19
  (6 other events, 66.6 us)
where the time goes:
time: 108 us
  waiting for transfers between devices  43.6 us (40%)
  starting transfers between devices  38.1 us (35%)
  Pallas kernels  23.9 us (22%)
  local copies, waits for them, and re-layouts  2.33 us (2%)
    ppermute x34, waiting for transfers between devices, swap(): return lax.ppermute(value, axis, [(i, i ^ bits) for i in range(n)])  43.6 us
    ppermute x34, starting transfers between devices, swap(): return lax.ppermute(value, axis, [(i, i ^ bits) for i in range(n)])  38.1 us
    pallas_call x4, Pallas kernels, ffn(): pl.pallas_call(functools.partial(ffn_kernel, n_tp=n_tp, rows=rows, block=...  16.1 us
    pallas_call x1, Pallas kernels, hold(): pl.pallas_call(hold_kernel, out_shape=[jax.ShapeDtypeStruct(w.shape, w.dt...  4.69 us
  transfers between devices with their start and end apart: 34, of which 15 were waited for; matrix products, arithmetic and copies ran while one was open for 1% of the time, Pallas kernels for 20%

commit v1 on v0

--- a/solution.py
+++ b/solution.py
@@ -103,19 +103,31 @@
     share_out[...] = columns[:, 2:4]
 
 
-def combine_kernel(target_ref, share_ref, *refs):
-    blocks, out, table = refs[:-2], refs[-2], refs[-1]
+def combine_kernel(target_ref, share_ref, *refs, first, n_blocks):
+    blocks, before, out, table = refs[:n_blocks], refs[n_blocks:-2], refs[-2], refs[-1]
     cap = blocks[0].shape[0]
     for k, block in enumerate(blocks):
         table[k * cap : (k + 1) * cap, :] = block[...]
-    rows = out.shape[0]
-    total = jnp.zeros(out.shape, jnp.float32)
-    slot = lax.broadcasted_iota(jnp.int32, (rows, table.shape[0]), 1)
+    slot = lax.broadcasted_iota(jnp.int32, (out.shape[0], table.shape[0]), 1) + first * cap
+    total = before[0][...] if before else jnp.zeros(out.shape, jnp.float32)
     for j in range(2):
         pick = (slot == target_ref[:, j : j + 1]).astype(jnp.float32).astype(jnp.bfloat16)
         found = jnp.dot(pick, table[...], preferred_element_type=jnp.float32)
         total = total + found * share_ref[:, j : j + 1]
-    out[...] = total.astype(jnp.bfloat16)
+    out[...] = total.astype(out.dtype)
+
+
+def combine(target, share, first, blocks, before, dtype):
+    cap, width = blocks[0].shape
+    return pl.pallas_call(
+        functools.partial(combine_kernel, first=first, n_blocks=len(blocks)),
+        out_shape=jax.ShapeDtypeStruct((target.shape[0], width), dtype),
+        in_specs=[VMEM] * (2 + len(blocks) + len(before)),
+        out_specs=VMEM,
+        scratch_shapes=[pltpu.VMEM((len(blocks) * cap, width), jnp.bfloat16)],
+        compiler_params=pltpu.CompilerParams(vmem_limit_bytes=8 * MIB),
+        name="combine",
+    )(target, share, *blocks, *before)
 
 
 def hold_kernel(*refs):
@@ -229,15 +241,8 @@
         for k, piece in zip(names, add_up(parts[0], size, group)):
             back[k] = swap(piece, "ep", k) if k else piece
 
-    return pl.pallas_call(
-        combine_kernel,
-        out_shape=jax.ShapeDtypeStruct((rows, width), jnp.bfloat16),
-        in_specs=[VMEM] * (2 + n_ep),
-        out_specs=VMEM,
-        scratch_shapes=[pltpu.VMEM((experts * cap, width), jnp.bfloat16)],
-        compiler_params=pltpu.CompilerParams(vmem_limit_bytes=8 * MIB),
-        name="combine",
-    )(target, share, *back)
+    most = combine(target, share, group, back[group:], [], jnp.float32)
+    return combine(target, share, 0, back[:group], [most], jnp.bfloat16)
 
 
 def solution(mesh):

time: 108 us -> 109 us (level)
  transfers between devices with their start and end apart: 34 -> 34, of which waited for: 15 -> 15; matrix products, arithmetic and copies ran while one was open for 1% -> 1% of each run, Pallas kernels for 20% -> 21%
where the time goes in v1:
time: 109 us; the launch traced here: 108 us
  waiting for transfers between devices  43.6 us (40%)
  starting transfers between devices  38.1 us (35%)
  Pallas kernels  24.1 us (22%)
  local copies, waits for them, and re-layouts  2.33 us (2%)
    ppermute x34, waiting for transfers between devices, swap(): return lax.ppermute(value, axis, [(i, i ^ bits) for i in range(n)])  43.6 us
    ppermute x34, starting transfers between devices, swap(): return lax.ppermute(value, axis, [(i, i ^ bits) for i in range(n)])  38.1 us
    pallas_call x4, Pallas kernels, ffn(): pl.pallas_call(functools.partial(ffn_kernel, n_tp=n_tp, rows=rows, block=...  16.1 us
    pallas_call x1, Pallas kernels, hold(): pl.pallas_call(hold_kernel, out_shape=[jax.ShapeDtypeStruct(w.shape, w.dt...  4.69 us
  transfers between devices with their start and end apart: 34, of which 15 were waited for; matrix products, arithmetic and copies ran while one was open for 1% of the time, Pallas kernels for 21%

profile of v1, /device:TPU:0, one launch (start us, length us, event | category | flops | bytes accessed | tf_op | source)
XLA Modules:
  0.0 108.3 jit_solution(4203489040688972423)
XLA Ops:
  2.2 3.1 %collective-permute-start = (bf16[128,512]{1,0:T(8,128)(2,1)S(1)}, bf16[128,512]{1,0:T(8,128)(2,1)S(1)}, u32[]{:S(2)}, u32[]{:S(2)}) collective-permute-start(bf16[128,512]{1,0:T(8,128)(2,1)S(1)} %get-tuple-element.41), channel_id=1, source_target_pairs={{0,4},{4,0},{8,12},{12,8},{16,20},{20,16},{24,28},{28,24},{1,5},{5... | collective-permute-start | bytes 393224 | tf_op jit(solution)/shard_map/ppermute | solution.py:19
  5.3 3.6 %collective-permute-start.25 = (bf16[128,512]{1,0:T(8,128)(2,1)S(1)}, bf16[128,512]{1,0:T(8,128)(2,1)S(1)}, u32[]{:S(2)}, u32[]{:S(2)}) collective-permute-start(bf16[128,512]{1,0:T(8,128)(2,1)S(1)} %get-tuple-element.61), channel_id=1, source_target_pairs={{0,24},{4,28},{8,16},{12,20},{16,8},{20,12},{24,0},{28,4},{1,25},{... | collective-permute-start | bytes 393224 | tf_op jit(solution)/shard_map/ppermute | solution.py:19
  9.6 1.7 %collective-permute-start.2 = (bf16[272,512]{1,0:T(8,128)(2,1)S(1)}, bf16[272,512]{1,0:T(8,128)(2,1)S(1)}, u32[]{:S(2)}, u32[]{:S(2)}) collective-permute-start(bf16[272,512]{1,0:T(8,128)(2,1)S(1)} %join.4.refs_0_.refs_4_), channel_id=1, source_target_pairs={{0,2},{1,3},{2,0},{3,1},{4,6},{5,7},{6,4},{7,5},{8,10},{9,11},{10,... | collective-permute-start | bytes 835592 | tf_op jit(solution)/shard_map/ppermute | solution.py:19
  11.3 2.8 %collective-permute-start.16 = (bf16[128,512]{1,0:T(8,128)(2,1)S(1)}, bf16[128,512]{1,0:T(8,128)(2,1)S(1)}, u32[]{:S(2)}, u32[]{:S(2)}) collective-permute-start(bf16[128,512]{1,0:T(8,128)(2,1)S(1)} %get-tuple-element.55), channel_id=1, source_target_pairs={{0,16},{4,20},{8,24},{12,28},{16,0},{20,4},{24,8},{28,12},{1,17},{... | collective-permute-start | bytes 393224 | tf_op jit(solution)/shard_map/ppermute | solution.py:19
  15.2 2.5 %collective-permute-done.26.refs_1_ = bf16[128,512]{1,0:T(8,128)(2,1)S(1)} collective-permute-done((bf16[128,512]{1,0:T(8,128)(2,1)S(1)}, bf16[128,512]{1,0:T(8,128)(2,1)S(1)}, u32[]{:S(2)}, u32[]{:S(2)}) %collective-permute-start.26) | collective-permute-done | bytes 131104 | tf_op jit(solution)/shard_map/ppermute | solution.py:19
  17.7 1.9 %collective-permute-start.28 = (bf16[256,512]{1,0:T(8,128)(2,1)S(1)}, bf16[256,512]{1,0:T(8,128)(2,1)S(1)}, u32[]{:S(2)}, u32[]{:S(2)}) collective-permute-start(bf16[256,512]{1,0:T(8,128)(2,1)S(1)} %join.7.refs_0_), channel_id=1, source_target_pairs={{0,2},{1,3},{2,0},{3,1},{4,6},{5,7},{6,4},{7,5},{8,10},{9,11},{10,... | collective-permute-start | bytes 786440 | tf_op jit(solution)/shard_map/ppermute | solution.py:19
  19.6 9.5 %collective-permute-done.16.refs_0_ = bf16[128,512]{1,0:T(8,128)(2,1)S(1)} collective-permute-done((bf16[128,512]{1,0:T(8,128)(2,1)S(1)}, bf16[128,512]{1,0:T(8,128)(2,1)S(1)}, u32[]{:S(2)}, u32[]{:S(2)}) %collective-permute-start.16) | collective-permute-done | bytes 131104 | tf_op jit(solution)/shard_map/ppermute | solution.py:19
  29.2 1.7 %collective-permute-done.17.refs_1_ = bf16[128,512]{1,0:T(8,128)(2,1)S(1)} collective-permute-done((bf16[128,512]{1,0:T(8,128)(2,1)S(1)}, bf16[128,512]{1,0:T(8,128)(2,1)S(1)}, u32[]{:S(2)}, u32[]{:S(2)}) %collective-permute-start.17) | collective-permute-done | bytes 131104 | tf_op jit(solution)/shard_map/ppermute | solution.py:19
  31.0 3.4 %collective-permute-done.7.refs_0_ = bf16[128,512]{1,0:T(8,128)(2,1)S(1)} collective-permute-done((bf16[128,512]{1,0:T(8,128)(2,1)S(1)}, bf16[128,512]{1,0:T(8,128)(2,1)S(1)}, u32[]{:S(2)}, u32[]{:S(2)}) %collective-permute-start.7) | collective-permute-done | bytes 131104 | tf_op jit(solution)/shard_map/ppermute | solution.py:19
  35.0 1.8 %collective-permute-done.8.refs_1_ = bf16[128,512]{1,0:T(8,128)(2,1)S(1)} collective-permute-done((bf16[128,512]{1,0:T(8,128)(2,1)S(1)}, bf16[128,512]{1,0:T(8,128)(2,1)S(1)}, u32[]{:S(2)}, u32[]{:S(2)}) %collective-permute-start.8) | collective-permute-done | bytes 131104 | tf_op jit(solution)/shard_map/ppermute | solution.py:19
  36.8 1.6 %collective-permute-start.19 = (bf16[256,512]{1,0:T(8,128)(2,1)S(1)}, bf16[256,512]{1,0:T(8,128)(2,1)S(1)}, u32[]{:S(2)}, u32[]{:S(2)}) collective-permute-start(bf16[256,512]{1,0:T(8,128)(2,1)S(1)} %join.6.refs_0_), channel_id=1, source_target_pairs={{0,2},{1,3},{2,0},{3,1},{4,6},{5,7},{6,4},{7,5},{8,10},{9,11},{10,... | collective-permute-start | bytes 786440 | tf_op jit(solution)/shard_map/ppermute | solution.py:19
  38.9 4.7 %hold.1 = (bf16[2048,1024]{1,0:T(8,128)(2,1)S(1)}, bf16[2048,1024]{1,0:T(8,128)(2,1)S(1)}, bf16[1024,2048]{1,0:T(8,128)(2,1)S(1)}) custom-call(bf16[2048,1024]{1,0:T(8,128)(2,1)} %bitcast.10, bf16[2048,1024]{1,0:T(8,128)(2,1)} %bitcast.11, bf16[1024,2048]{1,0:T(8,128)(2,1)} %bitcast.12), custom_call_target="tpu_custom_call" | custom-call | tf_op jit(solution)/shard_map/hold/pallas_call | solution.py:142
  43.6 2.4 %collective-permute-done.19.refs_2_ = bf16[256,512]{1,0:T(8,128)(2,1)S(1)} collective-permute-done((bf16[256,512]{1,0:T(8,128)(2,1)S(1)}, bf16[256,512]{1,0:T(8,128)(2,1)S(1)}, u32[]{:S(2)}, u32[]{:S(2)}) %collective-permute-start.19) | collective-permute-done | bytes 262176 | tf_op jit(solution)/shard_map/ppermute | solution.py:19
  45.9 3.4 %collective-permute-done.10.refs_2_ = bf16[256,512]{1,0:T(8,128)(2,1)S(1)} collective-permute-done((bf16[256,512]{1,0:T(8,128)(2,1)S(1)}, bf16[256,512]{1,0:T(8,128)(2,1)S(1)}, u32[]{:S(2)}, u32[]{:S(2)}) %collective-permute-start.10) | collective-permute-done | bytes 262176 | tf_op jit(solution)/shard_map/ppermute | solution.py:19
  49.9 4.0 %ffn.7 = (bf16[512,512]{1,0:T(8,128)(2,1)S(1)}, bf16[512,512]{1,0:T(8,128)(2,1)S(1)}) custom-call(s32[1]{0:T(128)} %bitcast.1.me_ref, bf16[256,512]{1,0:T(8,128)(2,1)S(1)} %join.7.refs_0_, bf16[256,512]{1,0:T(8,128)(2,1)S(1)} %collective-permute-done.27.refs_1_, bf16[256,512]{1,0:T(8,128)(2,1)S(1)} %collective-permute-done.28.refs_2_, ...), custom_call_target="tpu_custom_call" | custom-call | flops 3221225472 | bytes 12582912 | tf_op jit(solution)/shard_map/ffn/pallas_call | solution.py:184
  54.4 4.0 %ffn.6 = (bf16[512,512]{1,0:T(8,128)(2,1)S(1)}, bf16[512,512]{1,0:T(8,128)(2,1)S(1)}) custom-call(s32[1]{0:T(128)} %bitcast.1.me_ref, bf16[256,512]{1,0:T(8,128)(2,1)S(1)} %join.6.refs_0_, bf16[256,512]{1,0:T(8,128)(2,1)S(1)} %collective-permute-done.18.refs_1_, bf16[256,512]{1,0:T(8,128)(2,1)S(1)} %collective-permute-done.19.refs_2_, ...), custom_call_target="tpu_custom_call" | custom-call | flops 3221225472 | bytes 12582912 | tf_op jit(solution)/shard_map/ffn/pallas_call | solution.py:184
  58.6 4.0 %ffn.5 = (bf16[512,512]{1,0:T(8,128)(2,1)S(1)}, bf16[512,512]{1,0:T(8,128)(2,1)S(1)}) custom-call(s32[1]{0:T(128)} %bitcast.1.me_ref, bf16[256,512]{1,0:T(8,128)(2,1)S(1)} %join.5.refs_0_, bf16[256,512]{1,0:T(8,128)(2,1)S(1)} %collective-permute-done.9.refs_1_, bf16[256,512]{1,0:T(8,128)(2,1)S(1)} %collective-permute-done.10.refs_2_, ...), custom_call_target="tpu_custom_call" | custom-call | flops 3221225472 | bytes 12582912 | tf_op jit(solution)/shard_map/ffn/pallas_call | solution.py:184
  63.1 4.2 %ffn.4 = (bf16[512,512]{1,0:T(8,128)(2,1)S(1)}, bf16[512,512]{1,0:T(8,128)(2,1)S(1)}) custom-call(s32[1]{0:T(128)} %bitcast.1.me_ref, bf16[272,512]{1,0:T(8,128)(2,1)S(1)} %join.4.refs_0_.refs_4_, bf16[272,512]{1,0:T(8,128)(2,1)S(1)} %collective-permute-done.1.refs_1_.refs_5_, bf16[272,512]{1,0:T(8,128)(2,1)S(1)} %collective-permute-done.2.refs_2_.refs_6_, ...), custom_call_target="tpu_custom_call" | custom-call | flops 3221225472 | bytes 12582912 | tf_op jit(solution)/shard_map/ffn/pallas_call | solution.py:184
  67.4 1.3 %collective-permute-start.31 = (bf16[256,512]{1,0:T(8,128)(2,1)S(1)}, bf16[256,512]{1,0:T(8,128)(2,1)S(1)}, u32[]{:S(2)}, u32[]{:S(2)}) collective-permute-start(bf16[256,512]{1,0:T(8,128)(2,1)S(1)} %sum.14), channel_id=1, source_target_pairs={{0,2},{1,3},{2,0},{3,1},{4,6},{5,7},{6,4},{7,5},{8,10},{9,11},{10,... | collective-permute-start | bytes 786440 | tf_op jit(solution)/shard_map/ppermute | solution.py:19
  69.8 1.3 %collective-permute-start.13 = (bf16[256,512]{1,0:T(8,128)(2,1)S(1)}, bf16[256,512]{1,0:T(8,128)(2,1)S(1)}, u32[]{:S(2)}, u32[]{:S(2)}) collective-permute-start(bf16[256,512]{1,0:T(8,128)(2,1)S(1)} %sum.10), channel_id=1, source_target_pairs={{0,2},{1,3},{2,0},{3,1},{4,6},{5,7},{6,4},{7,5},{8,10},{9,11},{10,... | collective-permute-start | bytes 786440 | tf_op jit(solution)/shard_map/ppermute | solution.py:19
  72.0 4.7 %collective-permute-done.31.refs_2_ = bf16[256,512]{1,0:T(8,128)(2,1)S(1)} collective-permute-done((bf16[256,512]{1,0:T(8,128)(2,1)S(1)}, bf16[256,512]{1,0:T(8,128)(2,1)S(1)}, u32[]{:S(2)}, u32[]{:S(2)}) %collective-permute-start.31) | collective-permute-done | bytes 262176 | tf_op jit(solution)/shard_map/ppermute | solution.py:19
  76.8 3.3 %collective-permute-start.32 = (bf16[128,512]{1,0:T(8,128)(2,1)S(1)}, bf16[128,512]{1,0:T(8,128)(2,1)S(1)}, u32[]{:S(2)}, u32[]{:S(2)}) collective-permute-start(bf16[128,512]{1,0:T(8,128)(2,1)S(1)} %get-tuple-element.65), channel_id=1, source_target_pairs={{0,24},{4,28},{8,16},{12,20},{16,8},{20,12},{24,0},{28,4},{1,25},{... | collective-permute-start | bytes 393224 | tf_op jit(solution)/shard_map/ppermute | solution.py:19
  80.1 1.3 %collective-permute-start.33 = (bf16[128,512]{1,0:T(8,128)(2,1)S(1)}, bf16[128,512]{1,0:T(8,128)(2,1)S(1)}, u32[]{:S(2)}, u32[]{:S(2)}) collective-permute-start(bf16[128,512]{1,0:T(8,128)(2,1)S(1)} %get-tuple-element.66), channel_id=1, source_target_pairs={{0,28},{4,24},{8,20},{12,16},{16,12},{20,8},{24,4},{28,0},{1,29},{... | collective-permute-start | bytes 393224 | tf_op jit(solution)/shard_map/ppermute | solution.py:19
  82.4 3.7 %collective-permute-start.23 = (bf16[128,512]{1,0:T(8,128)(2,1)S(1)}, bf16[128,512]{1,0:T(8,128)(2,1)S(1)}, u32[]{:S(2)}, u32[]{:S(2)}) collective-permute-start(bf16[128,512]{1,0:T(8,128)(2,1)S(1)} %get-tuple-element.59), channel_id=1, source_target_pairs={{0,16},{4,20},{8,24},{12,28},{16,0},{20,4},{24,8},{28,12},{1,17},{... | collective-permute-start | bytes 393224 | tf_op jit(solution)/shard_map/ppermute | solution.py:19
  86.1 1.8 %collective-permute-done.13.refs_2_ = bf16[256,512]{1,0:T(8,128)(2,1)S(1)} collective-permute-done((bf16[256,512]{1,0:T(8,128)(2,1)S(1)}, bf16[256,512]{1,0:T(8,128)(2,1)S(1)}, u32[]{:S(2)}, u32[]{:S(2)}) %collective-permute-start.13) | collective-permute-done | bytes 262176 | tf_op jit(solution)/shard_map/ppermute | solution.py:19
  87.9 2.9 %collective-permute-start.24 = (bf16[128,512]{1,0:T(8,128)(2,1)S(1)}, bf16[128,512]{1,0:T(8,128)(2,1)S(1)}, u32[]{:S(2)}, u32[]{:S(2)}) collective-permute-start(bf16[128,512]{1,0:T(8,128)(2,1)S(1)} %get-tuple-element.60), channel_id=1, source_target_pairs={{0,20},{4,16},{8,28},{12,24},{16,4},{20,0},{24,12},{28,8},{1,21},{... | collective-permute-start | bytes 393224 | tf_op jit(solution)/shard_map/ppermute | solution.py:19
  90.9 2.1 %collective-permute-done.5.refs_2_ = bf16[256,512]{1,0:T(8,128)(2,1)S(1)} collective-permute-done((bf16[256,512]{1,0:T(8,128)(2,1)S(1)}, bf16[256,512]{1,0:T(8,128)(2,1)S(1)}, u32[]{:S(2)}, u32[]{:S(2)}) %collective-permute-start.5) | collective-permute-done | bytes 262176 | tf_op jit(solution)/shard_map/ppermute | solution.py:19
  93.0 2.2 %collective-permute-start.14 = (bf16[128,512]{1,0:T(8,128)(2,1)S(1)}, bf16[128,512]{1,0:T(8,128)(2,1)S(1)}, u32[]{:S(2)}, u32[]{:S(2)}) collective-permute-start(bf16[128,512]{1,0:T(8,128)(2,1)S(1)} %get-tuple-element.53), channel_id=1, source_target_pairs={{0,8},{4,12},{8,0},{12,4},{16,24},{20,28},{24,16},{28,20},{1,9},{5... | collective-permute-start | bytes 393224 | tf_op jit(solution)/shard_map/ppermute | solution.py:19
  97.3 3.1 %collective-permute-done.23.refs_2_ = bf16[128,512]{1,0:T(8,128)(2,1)S(1)} collective-permute-done((bf16[128,512]{1,0:T(8,128)(2,1)S(1)}, bf16[128,512]{1,0:T(8,128)(2,1)S(1)}, u32[]{:S(2)}, u32[]{:S(2)}) %collective-permute-start.23) | collective-permute-done | bytes 131104 | tf_op jit(solution)/shard_map/ppermute | solution.py:19
  100.4 1.9 %collective-permute-done.24.refs_3_ = bf16[128,512]{1,0:T(8,128)(2,1)S(1)} collective-permute-done((bf16[128,512]{1,0:T(8,128)(2,1)S(1)}, bf16[128,512]{1,0:T(8,128)(2,1)S(1)}, u32[]{:S(2)}, u32[]{:S(2)}) %collective-permute-start.24) | collective-permute-done | bytes 131104 | tf_op jit(solution)/shard_map/ppermute | solution.py:19
  102.3 2.8 %collective-permute-done.14.refs_0_ = bf16[128,512]{1,0:T(8,128)(2,1)S(1)} collective-permute-done((bf16[128,512]{1,0:T(8,128)(2,1)S(1)}, bf16[128,512]{1,0:T(8,128)(2,1)S(1)}, u32[]{:S(2)}, u32[]{:S(2)}) %collective-permute-start.14) | collective-permute-done | bytes 131104 | tf_op jit(solution)/shard_map/ppermute | solution.py:19
  105.1 1.5 %collective-permute-done.15.refs_1_ = bf16[128,512]{1,0:T(8,128)(2,1)S(1)} collective-permute-done((bf16[128,512]{1,0:T(8,128)(2,1)S(1)}, bf16[128,512]{1,0:T(8,128)(2,1)S(1)}, u32[]{:S(2)}, u32[]{:S(2)}) %collective-permute-start.15) | collective-permute-done | bytes 131104 | tf_op jit(solution)/shard_map/ppermute | solution.py:19
  (66 shorter events, 14.5 us)
Async XLA Ops:
  2.2 6.7 %collective-permute-start = (bf16[128,512]{1,0:T(8,128)(2,1)S(1)}, bf16[128,512]{1,0:T(8,128)(2,1)S(1)}, u32[]{:S(2)}, u32[]{:S(2)}) collective-permute-start(bf16[128,512]{1,0:T(8,128)(2,1)S(1)} %get-tuple-element.41), channel_id=1, source_target_pairs={{0,4},{4,0},{8,12},{12,8},{16,20},{20,16},{24,28},{28,24},{1,5},{5... | collective-permute-start | bytes 393224 | tf_op jit(solution)/shard_map/ppermute | solution.py:19
  5.3 9.9 %collective-permute-start.25 = (bf16[128,512]{1,0:T(8,128)(2,1)S(1)}, bf16[128,512]{1,0:T(8,128)(2,1)S(1)}, u32[]{:S(2)}, u32[]{:S(2)}) collective-permute-start(bf16[128,512]{1,0:T(8,128)(2,1)S(1)} %get-tuple-element.61), channel_id=1, source_target_pairs={{0,24},{4,28},{8,16},{12,20},{16,8},{20,12},{24,0},{28,4},{1,25},{... | collective-permute-start | bytes 393224 | tf_op jit(solution)/shard_map/ppermute | solution.py:19
  8.9 8.8 %collective-permute-start.26 = (bf16[128,512]{1,0:T(8,128)(2,1)S(1)}, bf16[128,512]{1,0:T(8,128)(2,1)S(1)}, u32[]{:S(2)}, u32[]{:S(2)}) collective-permute-start(bf16[128,512]{1,0:T(8,128)(2,1)S(1)} %get-tuple-element.62), channel_id=1, source_target_pairs={{0,28},{4,24},{8,20},{12,16},{16,12},{20,8},{24,4},{28,0},{1,29},{... | collective-permute-start | bytes 393224 | tf_op jit(solution)/shard_map/ppermute | solution.py:19
  9.6 24.9 %collective-permute-start.2 = (bf16[272,512]{1,0:T(8,128)(2,1)S(1)}, bf16[272,512]{1,0:T(8,128)(2,1)S(1)}, u32[]{:S(2)}, u32[]{:S(2)}) collective-permute-start(bf16[272,512]{1,0:T(8,128)(2,1)S(1)} %join.4.refs_0_.refs_4_), channel_id=1, source_target_pairs={{0,2},{1,3},{2,0},{3,1},{4,6},{5,7},{6,4},{7,5},{8,10},{9,11},{10,... | collective-permute-start | bytes 835592 | tf_op jit(solution)/shard_map/ppermute | solution.py:19
  11.3 17.7 %collective-permute-start.16 = (bf16[128,512]{1,0:T(8,128)(2,1)S(1)}, bf16[128,512]{1,0:T(8,128)(2,1)S(1)}, u32[]{:S(2)}, u32[]{:S(2)}) collective-permute-start(bf16[128,512]{1,0:T(8,128)(2,1)S(1)} %get-tuple-element.55), channel_id=1, source_target_pairs={{0,16},{4,20},{8,24},{12,28},{16,0},{20,4},{24,8},{28,12},{1,17},{... | collective-permute-start | bytes 393224 | tf_op jit(solution)/shard_map/ppermute | solution.py:19
  14.1 16.8 %collective-permute-start.17 = (bf16[128,512]{1,0:T(8,128)(2,1)S(1)}, bf16[128,512]{1,0:T(8,128)(2,1)S(1)}, u32[]{:S(2)}, u32[]{:S(2)}) collective-permute-start(bf16[128,512]{1,0:T(8,128)(2,1)S(1)} %get-tuple-element.56), channel_id=1, source_target_pairs={{0,20},{4,16},{8,28},{12,24},{16,4},{20,0},{24,12},{28,8},{1,21},{... | collective-permute-start | bytes 393224 | tf_op jit(solution)/shard_map/ppermute | solution.py:19
  17.7 20.7 %collective-permute-start.28 = (bf16[256,512]{1,0:T(8,128)(2,1)S(1)}, bf16[256,512]{1,0:T(8,128)(2,1)S(1)}, u32[]{:S(2)}, u32[]{:S(2)}) collective-permute-start(bf16[256,512]{1,0:T(8,128)(2,1)S(1)} %join.7.refs_0_), channel_id=1, source_target_pairs={{0,2},{1,3},{2,0},{3,1},{4,6},{5,7},{6,4},{7,5},{8,10},{9,11},{10,... | collective-permute-start | bytes 786440 | tf_op jit(solution)/shard_map/ppermute | solution.py:19
  19.6 19.3 %collective-permute-start.27 = (bf16[256,512]{1,0:T(8,128)(2,1)S(1)}, bf16[256,512]{1,0:T(8,128)(2,1)S(1)}, u32[]{:S(2)}, u32[]{:S(2)}) collective-permute-start(bf16[256,512]{1,0:T(8,128)(2,1)S(1)} %join.7.refs_0_), channel_id=1, source_target_pairs={{0,1},{1,0},{2,3},{3,2},{4,5},{5,4},{6,7},{7,6},{8,9},{9,8},{10,11... | collective-permute-start | bytes 786440 | tf_op jit(solution)/shard_map/ppermute | solution.py:19
  29.1 5.4 %collective-permute-start.7 = (bf16[128,512]{1,0:T(8,128)(2,1)S(1)}, bf16[128,512]{1,0:T(8,128)(2,1)S(1)}, u32[]{:S(2)}, u32[]{:S(2)}) collective-permute-start(bf16[128,512]{1,0:T(8,128)(2,1)S(1)} %get-tuple-element.49), channel_id=1, source_target_pairs={{0,8},{4,12},{8,0},{12,4},{16,24},{20,28},{24,16},{28,20},{1,9},{5... | collective-permute-start | bytes 393224 | tf_op jit(solution)/shard_map/ppermute | solution.py:19
  30.9 5.9 %collective-permute-start.8 = (bf16[128,512]{1,0:T(8,128)(2,1)S(1)}, bf16[128,512]{1,0:T(8,128)(2,1)S(1)}, u32[]{:S(2)}, u32[]{:S(2)}) collective-permute-start(bf16[128,512]{1,0:T(8,128)(2,1)S(1)} %get-tuple-element.50), channel_id=1, source_target_pairs={{0,12},{4,8},{8,4},{12,0},{16,28},{20,24},{24,20},{28,16},{1,13},{... | collective-permute-start | bytes 393224 | tf_op jit(solution)/shard_map/ppermute | solution.py:19
  34.5 14.9 %collective-permute-start.1 = (bf16[272,512]{1,0:T(8,128)(2,1)S(1)}, bf16[272,512]{1,0:T(8,128)(2,1)S(1)}, u32[]{:S(2)}, u32[]{:S(2)}) collective-permute-start(bf16[272,512]{1,0:T(8,128)(2,1)S(1)} %join.4.refs_0_.refs_4_), channel_id=1, source_target_pairs={{0,1},{1,0},{2,3},{3,2},{4,5},{5,4},{6,7},{7,6},{8,9},{9,8},{10,11... | collective-permute-start | bytes 835592 | tf_op jit(solution)/shard_map/ppermute | solution.py:19
  34.5 15.4 %collective-permute-start.3 = (bf16[272,512]{1,0:T(8,128)(2,1)S(1)}, bf16[272,512]{1,0:T(8,128)(2,1)S(1)}, u32[]{:S(2)}, u32[]{:S(2)}) collective-permute-start(bf16[272,512]{1,0:T(8,128)(2,1)S(1)} %collective-permute-done.2.refs_2_.refs_6_), channel_id=1, source_target_pairs={{0,1},{1,0},{2,3},{3,2},{4,5},{5,4},{6,7},{7,6},{8,9},{9,8},{10,11... | collective-permute-start | bytes 835592 | tf_op jit(solution)/shard_map/ppermute | solution.py:19
  36.8 9.2 %collective-permute-start.19 = (bf16[256,512]{1,0:T(8,128)(2,1)S(1)}, bf16[256,512]{1,0:T(8,128)(2,1)S(1)}, u32[]{:S(2)}, u32[]{:S(2)}) collective-permute-start(bf16[256,512]{1,0:T(8,128)(2,1)S(1)} %join.6.refs_0_), channel_id=1, source_target_pairs={{0,2},{1,3},{2,0},{3,1},{4,6},{5,7},{6,4},{7,5},{8,10},{9,11},{10,... | collective-permute-start | bytes 786440 | tf_op jit(solution)/shard_map/ppermute | solution.py:19
  38.3 11.0 %collective-permute-start.10 = (bf16[256,512]{1,0:T(8,128)(2,1)S(1)}, bf16[256,512]{1,0:T(8,128)(2,1)S(1)}, u32[]{:S(2)}, u32[]{:S(2)}) collective-permute-start(bf16[256,512]{1,0:T(8,128)(2,1)S(1)} %join.5.refs_0_), channel_id=1, source_target_pairs={{0,2},{1,3},{2,0},{3,1},{4,6},{5,7},{6,4},{7,5},{8,10},{9,11},{10,... | collective-permute-start | bytes 786440 | tf_op jit(solution)/shard_map/ppermute | solution.py:19
  38.9 10.9 %collective-permute-start.29 = (bf16[256,512]{1,0:T(8,128)(2,1)S(1)}, bf16[256,512]{1,0:T(8,128)(2,1)S(1)}, u32[]{:S(2)}, u32[]{:S(2)}) collective-permute-start(bf16[256,512]{1,0:T(8,128)(2,1)S(1)} %collective-permute-done.28.refs_2_), channel_id=1, source_target_pairs={{0,1},{1,0},{2,3},{3,2},{4,5},{5,4},{6,7},{7,6},{8,9},{9,8},{10,11... | collective-permute-start | bytes 786440 | tf_op jit(solution)/shard_map/ppermute | solution.py:19
  45.9 8.5 %collective-permute-start.18 = (bf16[256,512]{1,0:T(8,128)(2,1)S(1)}, bf16[256,512]{1,0:T(8,128)(2,1)S(1)}, u32[]{:S(2)}, u32[]{:S(2)}) collective-permute-start(bf16[256,512]{1,0:T(8,128)(2,1)S(1)} %join.6.refs_0_), channel_id=1, source_target_pairs={{0,1},{1,0},{2,3},{3,2},{4,5},{5,4},{6,7},{7,6},{8,9},{9,8},{10,11... | collective-permute-start | bytes 786440 | tf_op jit(solution)/shard_map/ppermute | solution.py:19
  49.3 9.2 %collective-permute-start.9 = (bf16[256,512]{1,0:T(8,128)(2,1)S(1)}, bf16[256,512]{1,0:T(8,128)(2,1)S(1)}, u32[]{:S(2)}, u32[]{:S(2)}) collective-permute-start(bf16[256,512]{1,0:T(8,128)(2,1)S(1)} %join.5.refs_0_), channel_id=1, source_target_pairs={{0,1},{1,0},{2,3},{3,2},{4,5},{5,4},{6,7},{7,6},{8,9},{9,8},{10,11... | collective-permute-start | bytes 786440 | tf_op jit(solution)/shard_map/ppermute | solution.py:19
  49.8 8.7 %collective-permute-start.11 = (bf16[256,512]{1,0:T(8,128)(2,1)S(1)}, bf16[256,512]{1,0:T(8,128)(2,1)S(1)}, u32[]{:S(2)}, u32[]{:S(2)}) collective-permute-start(bf16[256,512]{1,0:T(8,128)(2,1)S(1)} %collective-permute-done.10.refs_2_), channel_id=1, source_target_pairs={{0,1},{1,0},{2,3},{3,2},{4,5},{5,4},{6,7},{7,6},{8,9},{9,8},{10,11... | collective-permute-start | bytes 786440 | tf_op jit(solution)/shard_map/ppermute | solution.py:19
  53.9 13.5 %collective-permute-start.30 = (bf16[512,512]{1,0:T(8,128)(2,1)S(1)}, bf16[512,512]{1,0:T(8,128)(2,1)S(1)}, u32[]{:S(2)}, u32[]{:S(2)}) collective-permute-start(bf16[512,512]{1,0:T(8,128)(2,1)S(1)} %get-tuple-element.64), channel_id=1, source_target_pairs={{0,1},{1,0},{2,3},{3,2},{4,5},{5,4},{6,7},{7,6},{8,9},{9,8},{10,11... | collective-permute-start | bytes 1572872 | tf_op jit(solution)/shard_map/ppermute | solution.py:19
  58.4 10.3 %collective-permute-start.21 = (bf16[512,512]{1,0:T(8,128)(2,1)S(1)}, bf16[512,512]{1,0:T(8,128)(2,1)S(1)}, u32[]{:S(2)}, u32[]{:S(2)}) collective-permute-start(bf16[512,512]{1,0:T(8,128)(2,1)S(1)} %get-tuple-element.58), channel_id=1, source_target_pairs={{0,1},{1,0},{2,3},{3,2},{4,5},{5,4},{6,7},{7,6},{8,9},{9,8},{10,11... | collective-permute-start | bytes 1572872 | tf_op jit(solution)/shard_map/ppermute | solution.py:19
  62.6 7.1 %collective-permute-start.12 = (bf16[512,512]{1,0:T(8,128)(2,1)S(1)}, bf16[512,512]{1,0:T(8,128)(2,1)S(1)}, u32[]{:S(2)}, u32[]{:S(2)}) collective-permute-start(bf16[512,512]{1,0:T(8,128)(2,1)S(1)} %get-tuple-element.52), channel_id=1, source_target_pairs={{0,1},{1,0},{2,3},{3,2},{4,5},{5,4},{6,7},{7,6},{8,9},{9,8},{10,11... | collective-permute-start | bytes 1572872 | tf_op jit(solution)/shard_map/ppermute | solution.py:19
  67.4 9.2 %collective-permute-start.31 = (bf16[256,512]{1,0:T(8,128)(2,1)S(1)}, bf16[256,512]{1,0:T(8,128)(2,1)S(1)}, u32[]{:S(2)}, u32[]{:S(2)}) collective-permute-start(bf16[256,512]{1,0:T(8,128)(2,1)S(1)} %sum.14), channel_id=1, source_target_pairs={{0,2},{1,3},{2,0},{3,1},{4,6},{5,7},{6,4},{7,5},{8,10},{9,11},{10,... | collective-permute-start | bytes 786440 | tf_op jit(solution)/shard_map/ppermute | solution.py:19
  68.8 13.5 %collective-permute-start.22 = (bf16[256,512]{1,0:T(8,128)(2,1)S(1)}, bf16[256,512]{1,0:T(8,128)(2,1)S(1)}, u32[]{:S(2)}, u32[]{:S(2)}) collective-permute-start(bf16[256,512]{1,0:T(8,128)(2,1)S(1)} %sum.12), channel_id=1, source_target_pairs={{0,2},{1,3},{2,0},{3,1},{4,6},{5,7},{6,4},{7,5},{8,10},{9,11},{10,... | collective-permute-start | bytes 786440 | tf_op jit(solution)/shard_map/ppermute | solution.py:19
  69.8 18.2 %collective-permute-start.13 = (bf16[256,512]{1,0:T(8,128)(2,1)S(1)}, bf16[256,512]{1,0:T(8,128)(2,1)S(1)}, u32[]{:S(2)}, u32[]{:S(2)}) collective-permute-start(bf16[256,512]{1,0:T(8,128)(2,1)S(1)} %sum.10), channel_id=1, source_target_pairs={{0,2},{1,3},{2,0},{3,1},{4,6},{5,7},{6,4},{7,5},{8,10},{9,11},{10,... | collective-permute-start | bytes 786440 | tf_op jit(solution)/shard_map/ppermute | solution.py:19
  71.1 21.9 %collective-permute-start.5 = (bf16[256,512]{1,0:T(8,128)(2,1)S(1)}, bf16[256,512]{1,0:T(8,128)(2,1)S(1)}, u32[]{:S(2)}, u32[]{:S(2)}) collective-permute-start(bf16[256,512]{1,0:T(8,128)(2,1)S(1)} %sum.8), channel_id=1, source_target_pairs={{0,2},{1,3},{2,0},{3,1},{4,6},{5,7},{6,4},{7,5},{8,10},{9,11},{10,... | collective-permute-start | bytes 786440 | tf_op jit(solution)/shard_map/ppermute | solution.py:19
  76.8 18.4 %collective-permute-start.32 = (bf16[128,512]{1,0:T(8,128)(2,1)S(1)}, bf16[128,512]{1,0:T(8,128)(2,1)S(1)}, u32[]{:S(2)}, u32[]{:S(2)}) collective-permute-start(bf16[128,512]{1,0:T(8,128)(2,1)S(1)} %get-tuple-element.65), channel_id=1, source_target_pairs={{0,24},{4,28},{8,16},{12,20},{16,8},{20,12},{24,0},{28,4},{1,25},{... | collective-permute-start | bytes 393224 | tf_op jit(solution)/shard_map/ppermute | solution.py:19
  80.1 15.7 %collective-permute-start.33 = (bf16[128,512]{1,0:T(8,128)(2,1)S(1)}, bf16[128,512]{1,0:T(8,128)(2,1)S(1)}, u32[]{:S(2)}, u32[]{:S(2)}) collective-permute-start(bf16[128,512]{1,0:T(8,128)(2,1)S(1)} %get-tuple-element.66), channel_id=1, source_target_pairs={{0,28},{4,24},{8,20},{12,16},{16,12},{20,8},{24,4},{28,0},{1,29},{... | collective-permute-start | bytes 393224 | tf_op jit(solution)/shard_map/ppermute | solution.py:19
  82.4 18.0 %collective-permute-start.23 = (bf16[128,512]{1,0:T(8,128)(2,1)S(1)}, bf16[128,512]{1,0:T(8,128)(2,1)S(1)}, u32[]{:S(2)}, u32[]{:S(2)}) collective-permute-start(bf16[128,512]{1,0:T(8,128)(2,1)S(1)} %get-tuple-element.59), channel_id=1, source_target_pairs={{0,16},{4,20},{8,24},{12,28},{16,0},{20,4},{24,8},{28,12},{1,17},{... | collective-permute-start | bytes 393224 | tf_op jit(solution)/shard_map/ppermute | solution.py:19
  87.9 14.4 %collective-permute-start.24 = (bf16[128,512]{1,0:T(8,128)(2,1)S(1)}, bf16[128,512]{1,0:T(8,128)(2,1)S(1)}, u32[]{:S(2)}, u32[]{:S(2)}) collective-permute-start(bf16[128,512]{1,0:T(8,128)(2,1)S(1)} %get-tuple-element.60), channel_id=1, source_target_pairs={{0,20},{4,16},{8,28},{12,24},{16,4},{20,0},{24,12},{28,8},{1,21},{... | collective-permute-start | bytes 393224 | tf_op jit(solution)/shard_map/ppermute | solution.py:19
  93.0 12.1 %collective-permute-start.14 = (bf16[128,512]{1,0:T(8,128)(2,1)S(1)}, bf16[128,512]{1,0:T(8,128)(2,1)S(1)}, u32[]{:S(2)}, u32[]{:S(2)}) collective-permute-start(bf16[128,512]{1,0:T(8,128)(2,1)S(1)} %get-tuple-element.53), channel_id=1, source_target_pairs={{0,8},{4,12},{8,0},{12,4},{16,24},{20,28},{24,16},{28,20},{1,9},{5... | collective-permute-start | bytes 393224 | tf_op jit(solution)/shard_map/ppermute | solution.py:19
  95.2 11.5 %collective-permute-start.15 = (bf16[128,512]{1,0:T(8,128)(2,1)S(1)}, bf16[128,512]{1,0:T(8,128)(2,1)S(1)}, u32[]{:S(2)}, u32[]{:S(2)}) collective-permute-start(bf16[128,512]{1,0:T(8,128)(2,1)S(1)} %get-tuple-element.54), channel_id=1, source_target_pairs={{0,12},{4,8},{8,4},{12,0},{16,28},{20,24},{24,20},{28,16},{1,13},{... | collective-permute-start | bytes 393224 | tf_op jit(solution)/shard_map/ppermute | solution.py:19
  95.8 11.5 %collective-permute-start.6 = (bf16[128,512]{1,0:T(8,128)(2,1)S(1)}, bf16[128,512]{1,0:T(8,128)(2,1)S(1)}, u32[]{:S(2)}, u32[]{:S(2)}) collective-permute-start(bf16[128,512]{1,0:T(8,128)(2,1)S(1)} %get-tuple-element.48), channel_id=1, source_target_pairs={{0,4},{4,0},{8,12},{12,8},{16,20},{20,16},{24,28},{28,24},{1,5},{5... | collective-permute-start | bytes 393224 | tf_op jit(solution)/shard_map/ppermute | solution.py:19
  (6 other events, 66.7 us)
